TPU v7x, 128 devices: a whole 4x4x4 slice. The times are simulated.
128 devices in a mesh: ep: 128 (over z, y, x, core).
Axes of the slice: x: 4, y: 4, z: 4, core: 2. Of those that a mesh axis runs over, the one named last changes fastest.
Arguments:
- tokens: bfloat16 [4096, 2048], P('ep'), may hold values from -6 to 6
- gain_mix: float32 [2048], replicated, may hold values from 0.1 to 1.9
- w_query: bfloat16 [2048, 384], replicated, may hold values from -0.125 to 0.125
- w_key: bfloat16 [2048, 384], replicated, may hold values from -0.125 to 0.125
- w_value: bfloat16 [2048, 768], replicated, may hold values from -0.125 to 0.125
- w_input_gate: bfloat16 [2048, 4], replicated, may hold values from -0.125 to 0.125
- w_forget_gate: bfloat16 [2048, 4], replicated, may hold values from -0.125 to 0.125
- bias_input: float32 [4], replicated, may hold values from -1 to 1
- bias_forget: float32 [4], replicated, may hold values from 0 to 5
- memory_cells: float32 [4096, 4, 96, 192], P('ep'), may hold values from -6 to 6
- normalizer: float32 [4096, 4, 96], P('ep'), may hold values from -6 to 6
- stabilizer: float32 [4096, 4], P('ep'), may hold values from -1 to 1
- w_mix_out: bfloat16 [768, 2048], replicated, may hold values from -0.21875 to 0.21875
- gain_mix_post: float32 [2048], replicated, may hold values from 0.1 to 1.9
- gain_ffn: float32 [2048], replicated, may hold values from 0.1 to 1.9
- w_router: bfloat16 [2048, 32], replicated, may hold values from -0.125 to 0.125
- routing: int32 [4096, 2], replicated, may hold values from 0 to 31, all different within a row; in each aligned block of 32 rows (0 to 31, 32 to 63, ...) at most 4 rows name the same one
- w_expert_gate: bfloat16 [128, 2048, 384], P('ep'), may hold values from -0.125 to 0.125
- w_expert_up: bfloat16 [128, 2048, 384], P('ep'), may hold values from -0.125 to 0.125
- w_expert_down: bfloat16 [128, 384, 2048], P('ep'), may hold values from -0.15625 to 0.15625
- gain_ffn_post: float32 [2048], replicated, may hold values from 0.1 to 1.9
Outputs:
- mixed: bfloat16 [4096, 2048], P('ep')
- cells_next: float32 [4096, 4, 96, 192], P('ep')
- normalizer_next: float32 [4096, 4, 96], P('ep')
- stabilizer_next: float32 [4096, 4], P('ep')
Inputs may be any that keep to these rules, and one draw needn't show every extreme that they name: `routing`: each row names 2 different experts. In the rows of one device (aligned blocks of 32 rows) no expert is named more than 4 times, a bound that some block reaches.
All inputs are finite; a program needn't handle non-finite values.
Results may differ from a plain program's by a relative error of at most 0.012.
Values may be sent and summed in bfloat16 or wider, within the bound.
A program may use at most 128 MiB of HBM per device.

v0:
```python
import jax
import jax.numpy as jnp
from jax import lax
from jax.sharding import PartitionSpec as P

epsilon = 1e-06


def normalize(values, gain):
    return values * lax.rsqrt(jnp.mean(values * values, axis=-1, keepdims=True) + epsilon) * gain


def rounded(values):
    return lax.optimization_barrier(values.astype(jnp.bfloat16)).astype(jnp.float32)


def cell_step(
    normed,
    w_query,
    w_key,
    w_value,
    w_input_gate,
    w_forget_gate,
    bias_input,
    bias_forget,
    memory_cells,
    normalizer,
    stabilizer,
):
    row_count, heads, key_size, value_size = memory_cells.shape
    query_rows = rounded(jnp.dot(normed, w_query, preferred_element_type=jnp.float32))
    query_rows = query_rows.reshape(row_count, heads, key_size) * key_size ** (-0.5)
    key_rows = rounded(jnp.dot(normed, w_key, preferred_element_type=jnp.float32)).reshape(
        row_count, heads, key_size
    )
    value_rows = rounded(jnp.dot(normed, w_value, preferred_element_type=jnp.float32)).reshape(
        row_count, heads, value_size
    )
    input_gate = jnp.dot(normed, w_input_gate, preferred_element_type=jnp.float32) + bias_input
    log_forget = jax.nn.log_sigmoid(
        jnp.dot(normed, w_forget_gate, preferred_element_type=jnp.float32) + bias_forget
    )
    carried = log_forget + stabilizer
    stab_next = jnp.maximum(carried, input_gate)
    keep_weight = jnp.exp(carried - stab_next)
    write_weight = jnp.exp(input_gate - stab_next)
    scaled_keys = write_weight[:, :, None] * key_rows
    cells_next = (
        keep_weight[:, :, None, None] * memory_cells
        + scaled_keys[:, :, :, None] * value_rows[:, :, None, :]
    )
    norm_next = keep_weight[:, :, None] * normalizer + scaled_keys
    numerator = jnp.einsum("bhd,bhde->bhe", query_rows, cells_next, precision=lax.Precision.HIGHEST)
    denominator = jnp.einsum("bhd,bhd->bh", query_rows, norm_next, precision=lax.Precision.HIGHEST)
    denominator = jnp.maximum(jnp.abs(denominator), jnp.exp(-stab_next))
    cell_out = (
        (numerator / denominator[:, :, None])
        .reshape(row_count, heads * value_size)
        .astype(jnp.bfloat16)
    )
    return (cell_out, cells_next, norm_next, stab_next)


def route_weights(rows_in, w_router, routes):
    logits = jnp.dot(rows_in, w_router, preferred_element_type=jnp.float32)
    onehot = routes[:, :, None] == jnp.arange(w_router.shape[1], dtype=jnp.int32)[None, None, :]
    chosen = jnp.sum(jnp.where(onehot, logits[:, None, :], 0.0), axis=-1)
    return jax.nn.sigmoid(chosen - chosen[:, ::-1])


def expert_quarter(row_block, gate_w, up_w, down_w):
    gate_part = jnp.dot(row_block, gate_w, preferred_element_type=jnp.float32)
    up_part = jnp.dot(row_block, up_w, preferred_element_type=jnp.float32)
    hidden = (jax.nn.silu(gate_part) * up_part).astype(jnp.bfloat16)
    return jnp.dot(hidden, down_w, preferred_element_type=jnp.float32).astype(jnp.bfloat16)


def body(
    tokens,
    gain_mix,
    w_query,
    w_key,
    w_value,
    w_input_gate,
    w_forget_gate,
    bias_input,
    bias_forget,
    memory_cells,
    normalizer,
    stabilizer,
    w_mix_out,
    gain_mix_post,
    gain_ffn,
    w_router,
    routing,
    w_expert_gate,
    w_expert_up,
    w_expert_down,
    gain_ffn_post,
):
    devices = lax.axis_size("ep")
    device_index = lax.axis_index("ep")
    seq_rows = tokens.shape[0]
    model_width = tokens.shape[1]
    experts = w_router.shape[1]
    group_size = devices // experts
    top_count = routing.shape[1]
    capacity = max(2, seq_rows * top_count * 2 // experts)
    residual = tokens.astype(jnp.float32)
    normed = normalize(residual, gain_mix).astype(jnp.bfloat16)
    cell_out, cells_next, norm_next, stab_next = cell_step(
        normed,
        w_query,
        w_key,
        w_value,
        w_input_gate,
        w_forget_gate,
        bias_input,
        bias_forget,
        memory_cells,
        normalizer,
        stabilizer,
    )
    mix_out = jnp.dot(cell_out, w_mix_out, preferred_element_type=jnp.float32)
    after_mix = (residual + normalize(mix_out, gain_mix_post)).astype(jnp.bfloat16)
    after_float = after_mix.astype(jnp.float32)
    expert_in = normalize(after_float, gain_ffn).astype(jnp.bfloat16)
    gate_w = w_expert_gate[0]
    up_w = w_expert_up[0]
    down_w = w_expert_down[0]
    own_routes = lax.dynamic_slice_in_dim(routing, device_index * seq_rows, seq_rows, 0)
    route_weight = route_weights(expert_in, w_router, own_routes)
    flat_routes = own_routes.reshape(-1)
    flat_hot = (flat_routes[:, None] == jnp.arange(experts, dtype=jnp.int32)[None, :]).astype(
        jnp.int32
    )
    slot_index = jnp.sum((jnp.cumsum(flat_hot, axis=0) - 1) * flat_hot, axis=1)
    position = flat_routes * capacity + slot_index
    dispatch = position[:, None] == jnp.arange(experts * capacity, dtype=jnp.int32)[None, :]
    repeated = jnp.repeat(expert_in, top_count, axis=0)
    outgoing = jnp.einsum(
        "rp,rd->pd", dispatch.astype(jnp.bfloat16), repeated, preferred_element_type=jnp.float32
    ).astype(jnp.bfloat16)
    outgoing = jnp.broadcast_to(
        outgoing.reshape(experts, 1, capacity, model_width),
        (experts, group_size, capacity, model_width),
    ).reshape(devices, capacity, model_width)
    arrived = lax.all_to_all(outgoing, "ep", split_axis=0, concat_axis=0, tiled=True)
    shape_in = arrived.shape
    computed = expert_quarter(arrived.reshape(-1, model_width), gate_w, up_w, down_w).reshape(
        shape_in
    )
    returned = lax.all_to_all(computed, "ep", split_axis=0, concat_axis=0, tiled=True)
    summed = jnp.sum(
        returned.astype(jnp.float32).reshape(experts, group_size, capacity, model_width), axis=1
    )
    summed = summed.reshape(experts * capacity, model_width)
    combine = jnp.where(dispatch, route_weight.reshape(-1)[:, None], 0.0)
    expert_rows = jnp.dot(combine, summed, precision=lax.Precision.HIGHEST)
    expert_sum = jnp.sum(expert_rows.reshape(seq_rows, top_count, model_width), axis=1)
    mixed = (after_float + normalize(expert_sum, gain_ffn_post)).astype(jnp.bfloat16)
    return (mixed, cells_next, norm_next, stab_next)


def solution(mesh):
    return jax.shard_map(
        body,
        mesh=mesh,
        in_specs=(
            P("ep", None),
            P(),
            P(),
            P(),
            P(),
            P(),
            P(),
            P(),
            P(),
            P("ep", None, None, None),
            P("ep", None, None),
            P("ep", None),
            P(),
            P(),
            P(),
            P(),
            P(),
            P("ep", None, None),
            P("ep", None, None),
            P("ep", None, None),
            P(),
        ),
        out_specs=(P("ep", None), P("ep", None, None, None), P("ep", None, None), P("ep", None)),
        check_vma=False,
    )
```

profile of v0, /device:TPU:1, one launch (start us, length us, event | category | flops | bytes accessed | tf_op | source)
XLA Modules:
  0.0 145.2 jit_solution(10868732899291032671)
XLA Ops:
  0.7 1.2 fusion.20
  1.9 1.9 %convolution_convert_fusion.4 = bf16[32,384]{1,0:T(8,128)(2,1)S(1)} fusion(bf16[2048,384]{1,0:T(8,128)(2,1)} %param.23, bf16[32,2048]{1,0:T(8,128)(2,1)} %param.21, f32[2048]{0:T(1024)} %param.22, f32[32]{0:T(128)S(1)} %add_rsqrt_fusion.3), kind=kOutput, calls=%fused_computation.14 | convolution fusion | flops 50606080 | bytes 1736832 | tf_op jit(solution)/shard_map/dot_general | solution.py:31
  3.8 0.1 reshape.149
  4.0 0.1 mul.166
  4.1 0.2 convolution_add_fusion
  4.3 0.2 subtract_exponential_fusion.1
  4.6 0.6 copy-done.13
  5.3 0.7 constant_dynamic-slice_fusion
  6.1 0.1 copy.50
  6.2 0.1 eq.61
  6.3 1.8 %convolution_convert_fusion.3 = bf16[32,384]{1,0:T(8,128)(2,1)S(1)} fusion(bf16[2048,384]{1,0:T(8,128)(2,1)} %param.24, bf16[32,2048]{1,0:T(8,128)(2,1)S(1)} %copy-done.2, f32[2048]{0:T(1024)S(1)} %copy-done.6, f32[32]{0:T(128)S(1)} %add_rsqrt_fusion.3), kind=kOutput, calls=%fused_computation.13 | convolution fusion | flops 50606080 | bytes 1736832 | tf_op jit(solution)/shard_map/dot_general | solution.py:33
  8.2 0.1 reduce_window_sum.11
  8.3 0.8 select_reduce_fusion.1
  9.2 1.2 multiply_add_fusion.3
  10.4 0.7 reshape.145
  11.1 3.2 %convolution_convert_fusion.2 = bf16[32,768]{1,0:T(8,128)(2,1)} fusion(bf16[2048,768]{1,0:T(8,128)(2,1)} %param.25, bf16[32,2048]{1,0:T(8,128)(2,1)S(1)} %copy-done.2, f32[2048]{0:T(1024)S(1)} %copy-done.6, f32[32]{0:T(128)} %copy-done.15), kind=kOutput, calls=%fused_computation.12 | convolution fusion | flops 100950016 | bytes 3334272 | tf_op jit(solution)/shard_map/dot_general | solution.py:36
  14.4 0.8 multiply_reduce_fusion.2
  15.2 0.7 copy.40
  15.9 0.9 reshape.146
  16.9 6.1 %multiply_add_fusion = f32[32,4,96,192]{3,2,1,0:T(8,128)S(1)} fusion(f32[32,4,96,192]{3,2,1,0:T(8,128)} %param.30, f32[32,4,192]{2,1,0:T(4,128)S(1)} %reshape.146, f32[32,4,96]{2,1,0:T(4,128)S(1)} %get-tuple-element.8, f32[32,4]{1,0:T(8,128)} %copy-done.4), kind=kLoop, calls=%fused_computation | loop fusion | flops 7077888 | bytes 19022336 | tf_op jit(solution)/shard_map/add | solution.py:49
  23.0 6.1 %fusion.46 = f32[32,4,1,192]{3,2,1,0:T(1,128)S(1)} fusion(f32[32,4,96,1]{2,3,1,0:T(1,128)S(1)} %bitcast.43, f32[32,4,96,192]{3,2,1,0:T(8,128)S(1)} %multiply_add_fusion), kind=kOutput, calls=%fused_computation.75 | convolution fusion | flops 28311552 | bytes 9584640 | tf_op jit(solution)/shard_map/bhd,bhde->bhe/dot_general | solution.py:53
  29.1 0.1 fusion.28
  29.2 0.1 convert_element_type.59
  29.4 0.7 multiply_reduce_fusion.1
  30.1 0.2 fusion.24
  30.4 0.1 fusion.26
  30.5 0.8 broadcast_in_dim.30
  31.3 1.7 %reshape.137 = bf16[64,2048]{1,0:T(8,128)(2,1)} reshape(bf16[32,2,2048]{2,1,0:T(2,128)(2,1)} %broadcast_in_dim.30) | data formatting | bytes 524288 | tf_op jit(solution)/shard_map/reshape | solution.py:140
  33.1 2.1 %convolution_convert_fusion.1 = bf16[128,2048]{1,0:T(8,128)(2,1)} fusion(bf16[64,2048]{1,0:T(8,128)(2,1)} %reshape.137, s32[64]{0:T(128)S(1)} %copy-done.18), kind=kOutput, calls=%fused_computation.3 | convolution fusion | flops 33824768 | bytes 786688 | tf_op jit(solution)/shard_map/rp,rd->pd/dot_general | solution.py:141
  35.2 2.0 %broadcast_in_dim.31 = bf16[32,4,2048]{2,1,0:T(4,128)(2,1)} reshape(bf16[128,2048]{1,0:T(8,128)(2,1)} %convolution_convert_fusion.1) | data formatting | bytes 1048576 | tf_op jit(solution)/shard_map/broadcast_in_dim | solution.py:144
  37.3 2.1 %broadcast_in_dim.32 = bf16[32,4,4,2048]{3,2,1,0:T(4,128)(2,1)S(1)} broadcast(bf16[32,4,2048]{2,1,0:T(4,128)(2,1)} %broadcast_in_dim.31), dimensions={0,2,3} | broadcast | bytes 2621440 | tf_op jit(solution)/shard_map/broadcast_in_dim | solution.py:144
  39.4 41.9 %all_to_all.10 = bf16[128,4,2048]{2,1,0:T(4,128)(2,1)} all-to-all(bf16[128,4,2048]{2,1,0:T(4,128)(2,1)S(1)} %bitcast.42), channel_id=1, replica_groups=mesh['ep'=128] {'ep'}, dimensions={0} | all-to-all | bytes 4194304 | tf_op jit(solution)/shard_map/all_to_all | solution.py:148
  81.2 3.9 %reshape.139 = bf16[512,2048]{1,0:T(8,128)(2,1)} reshape(bf16[128,4,2048]{2,1,0:T(4,128)(2,1)} %all_to_all.10) | data formatting | bytes 4194304 | tf_op jit(solution)/shard_map/reshape | solution.py:150
  85.2 4.2 %fusion.3 = f32[512,384]{1,0:T(8,128)} fusion(bf16[512,2048]{1,0:T(8,128)(2,1)} %reshape.139, bf16[1,2048,384]{2,1,0:T(8,128)(2,1)} %param.38), kind=kOutput, calls=%fused_computation.7 | convolution fusion | flops 805306368 | bytes 4456448 | tf_op jit(solution)/shard_map/dot_general | solution.py:72
  89.4 6.4 %convolution_convert_fusion = bf16[512,2048]{1,0:T(8,128)(2,1)} fusion(bf16[1,384,2048]{2,1,0:T(8,128)(2,1)} %param.40, bf16[512,2048]{1,0:T(8,128)(2,1)} %reshape.139, bf16[1,2048,384]{2,1,0:T(8,128)(2,1)} %param.39, f32[512,384]{1,0:T(8,128)} %fusion.3), kind=kOutput, calls=%fused_computation.2 | convolution fusion | flops 1612840960 | bytes 8126464 | tf_op jit(solution)/shard_map/dot_general | solution.py:75
  95.8 4.1 %reshape.140 = bf16[128,4,2048]{2,1,0:T(4,128)(2,1)} reshape(bf16[512,2048]{1,0:T(8,128)(2,1)} %convolution_convert_fusion) | data formatting | bytes 4194304 | tf_op jit(solution)/shard_map/reshape | solution.py:150
  99.9 5.6 %all-to-all-start.1 = ((bf16[128,4,2048]{2,1,0:T(4,128)(2,1)}), bf16[128,4,2048]{2,1,0:T(4,128)(2,1)}, u32[]{:S(2)}, u32[]{:S(2)}) async-start(bf16[128,4,2048]{2,1,0:T(4,128)(2,1)} %reshape.140), calls=%async_computation.1 | async-start | bytes 4194304 | tf_op jit(solution)/shard_map/all_to_all | solution.py:153
  105.5 1.4 reduce_sum.77
  106.9 1.3 multiply_add_fusion.2
  108.2 0.8 copy.42
  109.0 0.2 fusion.47
  109.2 0.8 select_reduce_fusion
  110.1 25.7 %all-to-all-done.1 = bf16[128,4,2048]{2,1,0:T(4,128)(2,1)} async-done(((bf16[128,4,2048]{2,1,0:T(4,128)(2,1)}), bf16[128,4,2048]{2,1,0:T(4,128)(2,1)}, u32[]{:S(2)}, u32[]{:S(2)}) %all-to-all-start.1) | async-done | bytes 2097184 | tf_op jit(solution)/shard_map/all_to_all | solution.py:153
  135.8 4.0 %convert_reduce_fusion = f32[32,4,2048]{2,1,0:T(4,128)} fusion(bf16[128,4,2048]{2,1,0:T(4,128)(2,1)} %all-to-all-done.1), kind=kLoop, calls=%fused_computation.1 | loop fusion | flops 1835008 | bytes 3145728 | tf_op jit(solution)/shard_map/reduce_sum | solution.py:154
  139.8 2.6 %reshape.153 = f32[128,2048,1]{1,0,2:T(8,128)} reshape(f32[32,4,2048]{2,1,0:T(4,128)} %convert_reduce_fusion) | data formatting | bytes 2097152 | tf_op jit(solution)/shard_map/reshape | solution.py:157
  142.3 1.9 %convolution_reduce_fusion = f32[32,2048]{1,0:T(8,128)S(1)} fusion(f32[128,2048,1]{1,0,2:T(8,128)} %reshape.153, f32[32,2]{0,1:T(2,128)S(1)} %add_divide_fusion, s32[32,2]{0,1:T(2,128)S(1)} %copy.42), kind=kOutput, calls=%fused_computation.11 | convolution fusion | flops 201408512 | bytes 1311232 | tf_op jit(solution)/shard_map/dot_general | solution.py:159
  144.3 0.1 multiply_reduce_fusion
  144.4 0.8 fusion.27
  (60 shorter events, 0.5 us)
Async XLA Ops:
  0.6 28.7 %copy-start = (bf16[768,2048]{1,0:T(8,128)(2,1)S(1)}, bf16[768,2048]{1,0:T(8,128)(2,1)}, u32[]{:S(2)}) copy-start(bf16[768,2048]{1,0:T(8,128)(2,1)} %param.33) | copy-start | bytes 9437188
  0.6 3.4 %copy-start.2 = (bf16[32,2048]{1,0:T(8,128)(2,1)S(1)}, bf16[32,2048]{1,0:T(8,128)(2,1)}, u32[]{:S(2)}) copy-start(bf16[32,2048]{1,0:T(8,128)(2,1)} %param.21) | copy-start | bytes 393220
  0.7 3.4 %copy-start.6 = (f32[2048]{0:T(1024)S(1)}, f32[2048]{0:T(1024)}, u32[]{:S(2)}) copy-start(f32[2048]{0:T(1024)} %param.22) | copy-start | bytes 24580
  0.7 3.4 %copy-start.22 = (f32[4]{0:T(128)S(1)}, f32[4]{0:T(128)}, u32[]{:S(2)}) copy-start(f32[4]{0:T(128)} %param.28) | copy-start | bytes 52
  0.7 3.4 %copy-start.19 = (bf16[2048,4]{0,1:T(4,128)(2,1)S(1)}, bf16[2048,4]{0,1:T(4,128)(2,1)}, u32[]{:S(2)}) copy-start(bf16[2048,4]{0,1:T(4,128)(2,1)} %param.26) | copy-start | bytes 49156
  0.7 3.6 %copy-start.21 = (f32[32,4]{0,1:T(4,128)S(1)}, f32[32,4]{0,1:T(4,128)}, u32[]{:S(2)}) copy-start(f32[32,4]{0,1:T(4,128)} %param.32) | copy-start | bytes 1540
  0.7 3.6 %copy-start.23 = (f32[4]{0:T(128)S(1)}, f32[4]{0:T(128)}, u32[]{:S(2)}) copy-start(f32[4]{0:T(128)} %param.29) | copy-start | bytes 52
  0.7 3.6 %copy-start.20 = (bf16[2048,4]{0,1:T(4,128)(2,1)S(1)}, bf16[2048,4]{0,1:T(4,128)(2,1)}, u32[]{:S(2)}) copy-start(bf16[2048,4]{0,1:T(4,128)(2,1)} %param.27) | copy-start | bytes 49156
  1.9 4.4 %copy-start.15 = (f32[32]{0:T(128)}, f32[32]{0:T(128)S(1)}, u32[]{:S(2)}) copy-start(f32[32]{0:T(128)S(1)} %add_rsqrt_fusion.3) | copy-start | bytes 388
  4.6 0.6 copy-start.13
  5.3 9.1 %copy-start.4 = (f32[32,4]{1,0:T(8,128)}, f32[32,4]{1,0:T(8,128)S(1)}, u32[]{:S(2)}) copy-start(f32[32,4]{1,0:T(8,128)S(1)} %copy.37) | copy-start | bytes 1540
  6.1 2.0 %copy-start.9 = (s32[32,2]{0,1:T(2,128)}, s32[32,2]{0,1:T(2,128)S(1)}, u32[]{:S(2)}) copy-start(s32[32,2]{0,1:T(2,128)S(1)} %constant_dynamic-slice_fusion) | copy-start | bytes 772
  6.3 1.8 %copy-start.16 = (s32[64]{0:T(128)}, s32[64]{0:T(128)S(1)}, u32[]{:S(2)}) copy-start(s32[64]{0:T(128)S(1)} %eq.61) | copy-start | bytes 772
  9.1 2.0 %copy-start.17 = (s32[64]{0:T(128)}, s32[64]{0:T(128)S(1)}, u32[]{:S(2)}) copy-start(s32[64]{0:T(128)S(1)} %select_reduce_fusion.1) | copy-start | bytes 772
  9.2 6.0 %copy-start.14 = (f32[32,4]{0,1:T(4,128)S(1)}, f32[32,4]{0,1:T(4,128)}, u32[]{:S(2)}) copy-start(f32[32,4]{0,1:T(4,128)} %copy-done.13) | copy-start | bytes 1540
  11.1 3.3 %copy-start.3 = (f32[32,4,96]{2,1,0:T(4,128)S(1)}, f32[32,4,96]{2,1,0:T(4,128)}, u32[]{:S(2)}) copy-start(f32[32,4,96]{2,1,0:T(4,128)} %reshape.145) | copy-start | bytes 147460
  11.1 3.3 %copy-start.7 = (f32[32,4,96]{2,1,0:T(4,128)S(1)}, f32[32,4,96]{2,1,0:T(4,128)}, u32[]{:S(2)}) copy-start(f32[32,4,96]{2,1,0:T(4,128)} %param.31) | copy-start | bytes 147460
  23.0 6.1 %copy-start.1 = (f32[32,4,96,192]{3,2,1,0:T(8,128)}, f32[32,4,96,192]{3,2,1,0:T(8,128)S(1)}, u32[]{:S(2)}) copy-start(f32[32,4,96,192]{3,2,1,0:T(8,128)S(1)} %multiply_add_fusion) | copy-start | bytes 28311556
  23.0 6.1 %copy-start.8 = (f32[32,4]{1,0:T(8,128)S(1)}, f32[32,4]{1,0:T(8,128)}, u32[]{:S(2)}) copy-start(f32[32,4]{1,0:T(8,128)} %copy.40) | copy-start | bytes 1540
  29.1 1.0 copy-start.10
  29.2 1.2 copy-start.12
  29.3 3.7 %copy-start.18 = (s32[64]{0:T(128)S(1)}, s32[64]{0:T(128)}, u32[]{:S(2)}) copy-start(s32[64]{0:T(128)} %multiply_add_fusion.3) | copy-start | bytes 772
  99.9 9.1 %copy-start.5 = (bf16[2048,32]{0,1:T(8,128)(2,1)S(1)}, bf16[2048,32]{0,1:T(8,128)(2,1)}, u32[]{:S(2)}) copy-start(bf16[2048,32]{0,1:T(8,128)(2,1)} %param.36) | copy-start | bytes 393220
  99.9 35.9 %all-to-all-start.1 = ((bf16[128,4,2048]{2,1,0:T(4,128)(2,1)}), bf16[128,4,2048]{2,1,0:T(4,128)(2,1)}, u32[]{:S(2)}, u32[]{:S(2)}) async-start(bf16[128,4,2048]{2,1,0:T(4,128)(2,1)} %reshape.140), calls=%async_computation.1 | async-start | bytes 4194304 | tf_op jit(solution)/shard_map/all_to_all | solution.py:153
  139.8 4.6 %copy-start.11 = (f32[2048]{0:T(1024)S(1)}, f32[2048]{0:T(1024)}, u32[]{:S(2)}) copy-start(f32[2048]{0:T(1024)} %param.41) | copy-start | bytes 24580
where the time goes:
time: 146 us; the launch traced here: 145 us
  blocking collectives  41.9 us (29%)
  matrix products  29.1 us (20%)
  waiting for transfers between devices  25.7 us (18%)
  local copies, waits for them, and re-layouts  24.1 us (17%)
  other arithmetic  17.8 us (12%)
  starting transfers between devices  5.6 us (4%)
    all_to_all x1, blocking collectives, body(): lax.all_to_all(outgoing, 'ep', split_axis=0, concat_axis=0, tiled=True)  41.9 us
    all_to_all x1, waiting for transfers between devices, body(): lax.all_to_all(computed, 'ep', split_axis=0, concat_axis=0, tiled=True)  25.7 us
    dot_general x1, matrix products, expert_quarter(): jnp.dot(hidden, down_w, preferred_element_type=jnp.float32)  6.43 us
    add x1, other arithmetic, cell_step(): keep_weight[:, :, None, None] * memory_cells  6.1 us
    dot_general x1, matrix products, cell_step(): jnp.einsum('bhd,bhde->bhe', query_rows, cells_next, precision=lax.Precisi...  6.1 us
    all_to_all x1, starting transfers between devices, body(): lax.all_to_all(computed, 'ep', split_axis=0, concat_axis=0, tiled=True)  5.6 us
    dot_general x1, matrix products, expert_quarter(): gate_part = jnp.dot(row_block, gate_w, preferred_element_type=jnp.float32)  4.21 us
    broadcast_in_dim x2, local copies, waits for them, and re-layouts, body(): jnp.broadcast_to(outgoing.reshape(experts, 1, capacity, model_width), (ex...  4.12 us
  transfers between devices with their start and end apart: 1, of which 1 were waited for; matrix products, arithmetic and copies ran while one was open for 3% of the time, Pallas kernels for 0%

commit v1 on v0

v1 whole, which is shorter than its diff:
```python
import functools

import jax
import jax.numpy as jnp
from jax import lax
from jax.experimental import pallas as pl
from jax.experimental.pallas import tpu as pltpu
from jax.sharding import PartitionSpec as P

MESH = pl.DeviceIdType.MESH
F32, BF16 = jnp.float32, jnp.bfloat16
epsilon = 1e-06
VMEM_LIMIT = 64 * 1024 * 1024 - 64 * 1024

ROWS = 32
SLOTS = 4
CHIPS = 64
GROUPS = 4
PER = CHIPS // GROUPS
LANES = CHIPS * SLOTS
HALF = LANES // GROUPS
CHUNK = 4


def rms(values, gain):
    scale = lax.rsqrt(jnp.mean(values * values, axis=-1, keepdims=True) + epsilon)
    return values * scale * gain


def offset_of(index):
    g, dy, dx = index // PER, index // 4 % 4, index % 4
    return (g - dy - dx) % 4, dy, dx


def front_kernel(
    tok, gain_mix, wq, wk, wv, wi, wf, bias_i, bias_f, cells, norm, stab, wmix, gain_post, gain_ffn, wr, routes,
    cells_out, norm_out, stab_out, after_out, expert_out, weight_out, place_out,
    tok_v, gmix_v, wq_v, wk_v, wv_v, wi_v, wf_v, bi_v, bf_v, m_v, norm_v, stab_v, wmix_v, gpost_v, gffn_v, wr_v, rt_v,
    kt_v, qt_v, v_v, keep_v, write_v, num_v, den_v, t_v, in_sem, cell_sem, out_sem,
):
    me = lax.axis_index("ep")
    rows, heads, dk, dv = cells.shape
    chunks = rows // CHUNK
    t_v[...] = jnp.zeros_like(t_v)
    block = pl.multiple_of(me // 4 * 128, 128)
    pairs = [
        (tok, tok_v), (gain_mix, gmix_v), (wi, wi_v), (wf, wf_v), (bias_i, bi_v), (bias_f, bf_v), (stab, stab_v),
        (wq, wq_v), (wk, wk_v), (wv, wv_v), (norm, norm_v), (wmix, wmix_v), (gain_post, gpost_v), (gain_ffn, gffn_v),
        (wr, wr_v), (routes.at[:, pl.ds(block, 128)], rt_v),
    ]
    loads = [pltpu.make_async_copy(s, d, in_sem.at[i]) for i, (s, d) in enumerate(pairs)]

    def cell_load(ch):
        part = pl.ds(ch * CHUNK, CHUNK)
        return pltpu.make_async_copy(cells.at[part], m_v.at[part], cell_sem.at[ch])

    def cell_store(ch):
        part = pl.ds(ch * CHUNK, CHUNK)
        return pltpu.make_async_copy(m_v.at[part], cells_out.at[part], out_sem.at[ch])

    for copy in loads[:11]:
        copy.start()
    for ch in range(chunks):
        cell_load(ch).start()
    for copy in loads[11:]:
        copy.start()

    loads[0].wait()
    loads[1].wait()
    normed = rms(tok_v[...].astype(F32), gmix_v[...]).astype(BF16)

    for i in range(2, 7):
        loads[i].wait()
    nt = (((1,), (1,)), ((), ()))
    gate_in = lax.dot_general(normed, wi_v[...], nt, preferred_element_type=F32) + bi_v[...]
    forget = lax.dot_general(normed, wf_v[...], nt, preferred_element_type=F32) + bf_v[...]
    log_forget = jnp.minimum(forget, 0.0) - jnp.log1p(jnp.exp(-jnp.abs(forget)))
    t_v[0:heads, 0:rows] = stab_v[...]
    carried = log_forget + t_v[...].T[0:rows, 0:heads]
    stab_next = jnp.maximum(carried, gate_in)
    keep = jnp.exp(carried - stab_next)
    write = jnp.exp(gate_in - stab_next)
    floor = jnp.exp(-stab_next)
    for h in range(heads):
        keep_v[:, h, :] = jnp.broadcast_to(keep[:, h : h + 1], (rows, 128))
        write_v[:, h, :] = jnp.broadcast_to(write[:, h : h + 1], (rows, 128))
        t_v[0:rows, h : h + 1] = stab_next[:, h : h + 1]
    stab_out[...] = t_v[...].T[0:heads, 0:rows]

    loads[7].wait()
    query = jnp.dot(normed, wq_v[...], preferred_element_type=F32).astype(BF16).astype(F32)
    loads[8].wait()
    key = jnp.dot(normed, wk_v[...], preferred_element_type=F32).astype(BF16).astype(F32)
    pad = jnp.zeros((128 - rows, heads * dk), F32)
    qt_v[...] = jnp.concatenate([query, pad], axis=0).T
    kt_v[...] = jnp.concatenate([key, pad], axis=0).T
    loads[9].wait()
    value = jnp.dot(normed, wv_v[...], preferred_element_type=F32).astype(BF16).astype(F32)
    for h in range(heads):
        v_v[:, h, 0:dv] = value[:, dv * h : dv * h + dv]
    loads[10].wait()
    scale = dk ** (-0.5)
    for h in range(heads):
        fresh = keep[:, h : h + 1] * norm_v[:, h, :] + write[:, h : h + 1] * key[:, dk * h : dk * h + dk]
        norm_out[:, h, :] = fresh
        along = jnp.sum(query[:, dk * h : dk * h + dk] * scale * fresh, axis=-1, keepdims=True)
        den = jnp.maximum(jnp.abs(along), floor[:, h : h + 1])
        den_v[:, 128 * h : 128 * h + 128] = jnp.broadcast_to(den, (rows, 128))

    def serve(ch, carry):
        cell_load(ch).wait()
        shift = lax.rem(128 - ch * CHUNK, 128)
        for h in range(heads):
            kt = pltpu.roll(kt_v[dk * h : dk * h + dk, :], shift, 1)
            qt = pltpu.roll(qt_v[dk * h : dk * h + dk, :], shift, 1)
            for j in range(CHUNK):
                b = ch * CHUNK + j
                kc = jnp.broadcast_to(kt[:, j : j + 1], (dk, 128))
                qc = jnp.broadcast_to(qt[:, j : j + 1], (dk, 128))
                keep_b = keep_v[b, h : h + 1, :]
                write_b = write_v[b, h : h + 1, :]
                for lo, hi in ((0, 128), (128, dv)):
                    n = hi - lo
                    fed = write_b[:, :n] * v_v[b, h : h + 1, lo:hi]
                    fresh = keep_b[:, :n] * m_v[b, h, :, lo:hi] + kc[:, :n] * fed
                    m_v[b, h, :, lo:hi] = fresh
                    num_v[b, h : h + 1, lo:hi] = jnp.sum(qc[:, :n] * fresh, axis=0, keepdims=True)
        cell_store(ch).start()
        return carry

    lax.fori_loop(0, chunks, serve, 0)

    loads[11].wait()
    mix = jnp.zeros((rows, tok.shape[1]), F32)
    for h in range(heads):
        den = den_v[:, 128 * h : 128 * h + 128]
        wide = jnp.concatenate([den, den[:, : dv - 128]], axis=1)
        cell = (num_v[:, h, 0:dv] * scale / wide).astype(BF16)
        mix = mix + jnp.dot(cell, wmix_v[dv * h : dv * h + dv, :], preferred_element_type=F32)
    for i in range(12, 16):
        loads[i].wait()
    after = (tok_v[...].astype(F32) + rms(mix, gpost_v[...])).astype(BF16)
    after_out[...] = after
    expert_in = rms(after.astype(F32), gffn_v[...]).astype(BF16)
    expert_out[...] = expert_in

    t_v[...] = jnp.zeros_like(t_v)
    t_v[0:2, :] = rt_v[...].astype(F32)
    t_v[...] = t_v[...].T
    own = t_v[pl.ds(pl.multiple_of(lax.rem(me, 4) * rows, rows), rows), :]
    first, second = own[:, 0:1], own[:, 1:2]
    logits = lax.dot_general(expert_in, wr_v[...], nt, preferred_element_type=F32)
    ids = lax.broadcasted_iota(jnp.int32, logits.shape, 1).astype(F32)
    zero = jnp.zeros_like(logits)
    chosen0 = jnp.sum(jnp.where(ids == first, logits, zero), axis=-1, keepdims=True)
    chosen1 = jnp.sum(jnp.where(ids == second, logits, zero), axis=-1, keepdims=True)
    weight0 = jax.nn.sigmoid(chosen0 - chosen1)
    weight1 = jax.nn.sigmoid(chosen1 - chosen0)
    lane = lax.broadcasted_iota(jnp.int32, (rows, LANES), 1)
    index = lane >> 2
    dy, dx = (index >> 2) & 3, index & 3
    dz = ((index >> 4) - dy - dx + 8) & 3
    mine = me // 2
    cz = (mine // 16 + dz) & 3
    cy = (lax.rem(mine // 4, 4) + dy) & 3
    cx = (lax.rem(mine, 4) + dx) & 3
    expert = ((cz * 16 + cy * 4 + cx) >> 1).astype(F32)
    hit0 = (expert == first).astype(F32)
    hit1 = (expert == second).astype(F32)
    hot = hit0 + hit1
    before = lax.broadcasted_iota(jnp.int32, (rows, rows), 1) < lax.broadcasted_iota(jnp.int32, (rows, rows), 0)
    rank = jnp.dot(before.astype(F32).astype(BF16), hot.astype(BF16), preferred_element_type=F32)
    place = jnp.where(rank == (lane & 3).astype(F32), hot, 0.0)
    place_out[...] = place.astype(BF16)
    weight_out[...] = place * (hit0 * weight0 + hit1 * weight1)

    def drain(ch, carry):
        cell_store(ch).wait()
        return carry

    lax.fori_loop(0, chunks, drain, 0)


def expert_kernel(
    expert_in, after, weight, place, wg, wu, wd, gain_post,
    mixed,
    wg_v, wu_v, wd_v, send, xa, xb, own_part, part_send, part_recv, back_send, back,
    w_sem, send_s, send_r, fwd_s, fwd_r, part_s, part_r, back_s, back_r,
):
    me = lax.axis_index("ep")
    core, chip = lax.rem(me, 2), me // 2
    z, y, x = chip // 16, lax.rem(chip // 4, 4), lax.rem(chip, 4)
    partner = me + 1 - 2 * core

    def at(index, sign):
        dz, dy, dx = offset_of(index)
        if sign < 0:
            dz, dy, dx = -dz % 4, -dy % 4, -dx % 4
        return ((lax.rem(z + dz, 4) * 4 + lax.rem(y + dy, 4)) * 4 + lax.rem(x + dx, 4)) * 2 + core

    def cut(index):
        return pl.ds(SLOTS * index, SLOTS)

    barrier = pltpu.get_barrier_semaphore()
    for i in range(1, CHIPS):
        pl.semaphore_signal(barrier, inc=1, device_id=(at(i, 1),), device_id_type=MESH)
    pl.semaphore_signal(barrier, inc=1, device_id=(partner,), device_id_type=MESH)
    weights = [
        pltpu.make_async_copy(s.at[0], d, w_sem.at[i]) for i, (s, d) in enumerate(((wg, wg_v), (wu, wu_v), (wd, wd_v)))
    ]
    for copy in weights:
        copy.start()
    tn = (((0,), (0,)), ((), ()))
    send[...] = lax.dot_general(place[...], expert_in[...], tn, preferred_element_type=F32).astype(BF16)
    xa[0:SLOTS, :] = send[0:SLOTS, :]
    pl.semaphore_wait(barrier, CHIPS)

    def to_expert(i):
        return pltpu.make_async_remote_copy(
            src_ref=send.at[cut(i)], dst_ref=xa.at[cut(i)], send_sem=send_s.at[i], recv_sem=send_r.at[i],
            device_id=(at(i, 1),), device_id_type=MESH,
        )

    def to_source(i):
        return pltpu.make_async_remote_copy(
            src_ref=back_send.at[cut(i)], dst_ref=back.at[cut(i)], send_sem=back_s.at[i], recv_sem=back_r.at[i],
            device_id=(at(i, -1),), device_id_type=MESH,
        )

    def to_partner(src, dst, ssem, rsem, g):
        part = pl.ds(HALF * g, HALF)
        return pltpu.make_async_remote_copy(
            src_ref=src.at[part], dst_ref=dst.at[part], send_sem=ssem.at[g], recv_sem=rsem.at[g],
            device_id=(partner,), device_id_type=MESH,
        )

    order = list(range(GROUPS))[1:] + [0]
    for g in order:
        for i in range(PER * g, PER * g + PER):
            if i:
                to_expert(i).start()
    for copy in weights:
        copy.wait()

    def finish(g):
        part = slice(HALF * g, HALF * g + HALF)
        to_partner(part_send, part_recv, part_s, part_r, g).wait_recv()
        back_send[part, :] = (own_part[part, :] + part_recv[part, :].astype(F32)).astype(BF16)
        for i in range(PER * g, PER * g + PER):
            if i:
                to_source(i).start()
            else:
                back[0:SLOTS, :] = back_send[0:SLOTS, :]

    last = None
    for g in order:
        part = slice(HALF * g, HALF * g + HALF)
        for i in range(PER * g, PER * g + PER):
            if i:
                to_expert(i).wait_recv()
        to_partner(xa, xb, fwd_s, fwd_r, g).start()
        if last is not None:
            finish(last)
        to_partner(xa, xb, fwd_s, fwd_r, g).wait_recv()
        block = jnp.concatenate([xa[part, :], xb[part, :]], axis=0)
        gate = jnp.dot(block, wg_v[...], preferred_element_type=F32)
        up = jnp.dot(block, wu_v[...], preferred_element_type=F32)
        hidden = (gate * jax.nn.sigmoid(gate) * up).astype(BF16)
        result = jnp.dot(hidden, wd_v[...], preferred_element_type=F32)
        part_send[part, :] = result[HALF:, :].astype(BF16)
        to_partner(part_send, part_recv, part_s, part_r, g).start()
        own_part[part, :] = result[:HALF, :]
        last = g
    finish(last)

    total = None
    high = weight[...].astype(BF16)
    low = (weight[...] - high.astype(F32)).astype(BF16)
    for g in order:
        part = slice(HALF * g, HALF * g + HALF)
        for i in range(PER * g, PER * g + PER):
            if i:
                to_source(i).wait_recv()
        rows = back[part, :]
        more = jnp.dot(high[:, part], rows, preferred_element_type=F32)
        more = more + jnp.dot(low[:, part], rows, preferred_element_type=F32)
        total = more if total is None else total + more
    mixed[...] = (after[...].astype(F32) + rms(total, gain_post[...])).astype(BF16)

    for i in range(1, CHIPS):
        to_expert(i).wait_send()
        to_source(i).wait_send()
    for g in range(GROUPS):
        to_partner(xa, xb, fwd_s, fwd_r, g).wait_send()
        to_partner(part_send, part_recv, part_s, part_r, g).wait_send()


def body(
    tokens, gain_mix, w_query, w_key, w_value, w_input_gate, w_forget_gate, bias_input, bias_forget, memory_cells,
    normalizer, stabilizer, w_mix_out, gain_mix_post, gain_ffn, w_router, routing, w_expert_gate, w_expert_up,
    w_expert_down, gain_ffn_post,
):
    rows, width = tokens.shape
    _, heads, dk, dv = memory_cells.shape
    hidden = w_expert_gate.shape[2]
    row = lambda v: v.reshape(1, -1)
    front_in = (
        tokens, row(gain_mix), w_query, w_key, w_value, w_input_gate.T, w_forget_gate.T, row(bias_input),
        row(bias_forget), memory_cells, normalizer, stabilizer.T, w_mix_out, row(gain_mix_post), row(gain_ffn),
        w_router.T, routing.T,
    )
    anywhere, vmem = pl.BlockSpec(memory_space=pl.ANY), pl.BlockSpec(memory_space=pltpu.VMEM)
    shape = jax.ShapeDtypeStruct
    dma = pltpu.SemaphoreType.DMA
    scratch = [pltpu.VMEM(a.shape, a.dtype) for a in front_in]
    scratch[-1] = pltpu.VMEM((2, 128), jnp.int32)
    cells_next, norm_next, stab_next, after, expert_in, weight, place = pl.pallas_call(
        front_kernel,
        out_shape=(
            shape(memory_cells.shape, F32), shape(normalizer.shape, F32), shape((heads, rows), F32),
            shape((rows, width), BF16), shape((rows, width), BF16), shape((rows, LANES), F32), shape((rows, LANES), BF16),
        ),
        in_specs=[anywhere] * len(front_in),
        out_specs=(anywhere,) + (vmem,) * 6,
        scratch_shapes=scratch
        + [
            pltpu.VMEM((heads * dk, 128), F32), pltpu.VMEM((heads * dk, 128), F32), pltpu.VMEM((rows, heads, 256), F32),
            pltpu.VMEM((rows, heads, 128), F32), pltpu.VMEM((rows, heads, 128), F32),
            pltpu.VMEM((rows, heads, 256), F32), pltpu.VMEM((rows, heads * 128), F32), pltpu.VMEM((128, 128), F32),
            dma((16,)), dma((rows // CHUNK,)), dma((rows // CHUNK,)),
        ],
        compiler_params=pltpu.CompilerParams(vmem_limit_bytes=VMEM_LIMIT),
        name="front",
    )(*front_in)

    big = pltpu.VMEM((LANES, width), BF16)
    mixed = pl.pallas_call(
        expert_kernel,
        out_shape=shape((rows, width), BF16),
        in_specs=[vmem] * 4 + [anywhere] * 3 + [vmem],
        out_specs=vmem,
        scratch_shapes=[
            pltpu.VMEM((width, hidden), BF16), pltpu.VMEM((width, hidden), BF16), pltpu.VMEM((hidden, width), BF16),
            big, big, big, pltpu.VMEM((LANES, width), F32), big, big, big, big,
            dma((3,)), dma((CHIPS,)), dma((CHIPS,)), dma((GROUPS,)), dma((GROUPS,)), dma((GROUPS,)), dma((GROUPS,)),
            dma((CHIPS,)), dma((CHIPS,)),
        ],
        compiler_params=pltpu.CompilerParams(collective_id=0, has_side_effects=True, vmem_limit_bytes=VMEM_LIMIT),
        name="experts",
    )(expert_in, after, weight, place, w_expert_gate, w_expert_up, w_expert_down, row(gain_ffn_post))
    return (mixed, cells_next, norm_next, stab_next.T)


def solution(mesh):
    return jax.shard_map(
        body,
        mesh=mesh,
        in_specs=(
            P("ep", None),
            P(),
            P(),
            P(),
            P(),
            P(),
            P(),
            P(),
            P(),
            P("ep", None, None, None),
            P("ep", None, None),
            P("ep", None),
            P(),
            P(),
            P(),
            P(),
            P(),
            P("ep", None, None),
            P("ep", None, None),
            P("ep", None, None),
            P(),
        ),
        out_specs=(P("ep", None), P("ep", None, None, None), P("ep", None, None), P("ep", None)),
        check_vma=False,
    )
```

time: 146 us -> 61.2 us (0.42)
  Pallas kernels: 0 us -> 58.9 us
  blocking collectives: 41.9 us -> 0 us
  matrix products: 29.1 us -> 0 us
  waiting for transfers between devices: 25.7 us -> 0 us
  local copies, waits for them, and re-layouts: 24.1 us -> 1.57 us
  other arithmetic: 17.8 us -> 0 us
  starting transfers between devices: 5.6 us -> 0 us
    pallas_call x0 -> x2, Pallas kernels: none -> 58.9 us  [the longest x1 43 us: body(): pl.pallas_call(expert_kernel, out_shape=shape((rows, width), BF16), in_sp...]
    all_to_all x1 -> x0, blocking collectives: 41.9 us -> none  [body(): lax.all_to_all(outgoing, 'ep', split_axis=0, concat_axis=0, tiled=True)]
    dot_general x12 -> x0, matrix products: 29.1 us -> none  [the longest x1 6.43 us: expert_quarter(): jnp.dot(hidden, down_w, preferred_element_type=jnp.float32)]
    all_to_all x1 -> x0, waiting for transfers between devices: 25.7 us -> none  [body(): lax.all_to_all(computed, 'ep', split_axis=0, concat_axis=0, tiled=True)]
    reshape x5 -> x0, local copies, waits for them, and re-layouts: 13.1 us -> none  [the longest x1 4.11 us: body(): expert_quarter(arrived.reshape(-1, model_width), gate_w, up_w, down_w)]
    add x3 -> x0, other arithmetic: 8.62 us -> none  [the longest x1 6.1 us: cell_step(): keep_weight[:, :, None, None] * memory_cells]
    reduce_sum x6 -> x0, other arithmetic: 7.2 us -> none  [the longest x1 3.98 us: body(): jnp.sum(returned.astype(jnp.float32).reshape(experts, group_size, capacit...]
    all_to_all x1 -> x0, starting transfers between devices: 5.6 us -> none  [body(): lax.all_to_all(computed, 'ep', split_axis=0, concat_axis=0, tiled=True)]
  transfers between devices with their start and end apart: 1 -> 0, of which waited for: 1 -> 0; matrix products, arithmetic and copies ran while one was open for 3% -> 0% of each run, Pallas kernels for 0% -> 0%
where the time goes in v1:
time: 61.2 us; the launch traced here: 61.1 us
  Pallas kernels  58.9 us (96%)
  local copies, waits for them, and re-layouts  1.57 us (3%)
  between operations  0.65 us (1%)
    pallas_call x1, Pallas kernels, body(): pl.pallas_call(expert_kernel, out_shape=shape((rows, width), BF16), in_sp...  43 us
    pallas_call x1, Pallas kernels, body(): pl.pallas_call(front_kernel, out_shape=(shape(memory_cells.shape, F32), s...  15.9 us
    unnamed x1, local copies, waits for them, and re-layouts  1.57 us

profile of v1, /device:TPU:1, one launch (start us, length us, event | category | flops | bytes accessed | tf_op | source)
XLA Modules:
  0.0 61.1 jit_solution(17189452911055396543)
XLA Ops:
  0.6 15.9 %front.1 = (f32[32,4,96,192]{3,2,1,0:T(8,128)}, f32[32,4,96]{2,1,0:T(4,128)}, f32[4,32]{1,0:T(4,128)}, bf16[32,2048]{1,0:T(8,128)(2,1)}, bf16[32,2048]{1,0:T(8,1...) custom-call(bf16[32,2048]{1,0:T(8,128)(2,1)} %tok.1, f32[1,2048]{1,0:T(1,128)} %bitcast.16, bf16[2048,384]{1,0:T(8,128)(2,1)} %wq.1, ...), custom_call_target="tpu_custom_call" | custom-call | tf_op jit(solution)/shard_map/front/pallas_call | solution.py:317
  16.5 43.0 %experts.1 = bf16[32,2048]{1,0:T(8,128)(2,1)} custom-call(bf16[32,2048]{1,0:T(8,128)(2,1)} %get-tuple-element.11.expert_in, bf16[32,2048]{1,0:T(8,128)(2,1)} %get-tuple-element.12.after, f32[32,256]{1,0:T(8,128)} %get-tuple-element.13.weight, bf16[32,256]{1,0:T(8,128)(2,1)} %get-tuple-element.14.place, bf16[1,2048,384]{2,1,0:T(8,128)(2,1)} %wg.1, ...), custom_call_target="tpu_custom_call" | custom-call | tf_op jit(solution)/shard_map/experts/pallas_call | solution.py:337
  59.5 1.6 %copy.26 = bf16[32,2048]{1,0:T(8,128)(2,1)} copy(bf16[32,2048]{1,0:T(8,128)(2,1)} %experts.1) | data formatting | bytes 262144

commit v2 on v1

v2 whole, which is shorter than its diff:
```python
import functools

import jax
import jax.numpy as jnp
from jax import lax
from jax.experimental import pallas as pl
from jax.experimental.pallas import tpu as pltpu
from jax.sharding import PartitionSpec as P

MESH = pl.DeviceIdType.MESH
F32, BF16 = jnp.float32, jnp.bfloat16
epsilon = 1e-06
VMEM_LIMIT = 64 * 1024 * 1024 - 256 * 1024

ROWS = 32
SLOTS = 4
CHIPS = 64
GROUPS = 4
PER = CHIPS // GROUPS
LANES = CHIPS * SLOTS
HALF = LANES // GROUPS
NT = (((1,), (1,)), ((), ()))
CHUNK = 4


def rms(values, gain):
    scale = lax.rsqrt(jnp.mean(values * values, axis=-1, keepdims=True) + epsilon)
    return values * scale * gain


def offset_of(index):
    g, dy, dx = index // PER, index // 4 % 4, index % 4
    return (g - dy - dx) % 4, dy, dx


def front_kernel(
    tok, gain_mix, wq, wk, wv, wi, wf, bias_i, bias_f, cells, norm, stab,
    cells_out, norm_out, stab_out, cell_out,
    tok_v, gmix_v, wq_v, wk_v, wv_v, wi_v, wf_v, bi_v, bf_v, m_v, norm_v, stab_v,
    cell_v, kt_v, q_v, v_v, keep_v, write_v, num_v, den_v, t_v, in_sem, cell_sem, out_sem,
):
    rows, heads, dk, dv = cells.shape
    chunks = rows // CHUNK
    pairs = [
        (tok, tok_v), (gain_mix, gmix_v), (wi, wi_v), (wf, wf_v), (bias_i, bi_v), (bias_f, bf_v), (stab, stab_v),
        (wq, wq_v), (wk, wk_v), (wv, wv_v), (norm, norm_v),
    ]
    loads = [pltpu.make_async_copy(s, d, in_sem.at[i]) for i, (s, d) in enumerate(pairs)]

    def cell_load(ch):
        part = pl.ds(ch * CHUNK, CHUNK)
        return pltpu.make_async_copy(cells.at[part], m_v.at[part], cell_sem.at[ch])

    def cell_store(ch):
        part = pl.ds(ch * CHUNK, CHUNK)
        return pltpu.make_async_copy(m_v.at[part], cells_out.at[part], out_sem.at[ch])

    for copy in loads:
        copy.start()
    cell_load(0).start()

    t_v[...] = jnp.zeros_like(t_v)
    loads[0].wait()
    loads[1].wait()
    normed = rms(tok_v[...].astype(F32), gmix_v[...]).astype(BF16)

    for i in range(2, 7):
        loads[i].wait()
    gate_in = lax.dot_general(normed, wi_v[...], NT, preferred_element_type=F32) + bi_v[...]
    forget = lax.dot_general(normed, wf_v[...], NT, preferred_element_type=F32) + bf_v[...]
    log_forget = jnp.minimum(forget, 0.0) - jnp.log1p(jnp.exp(-jnp.abs(forget)))
    t_v[0:heads, 0:rows] = stab_v[...]
    carried = log_forget + t_v[...].T[0:rows, 0:heads]
    stab_next = jnp.maximum(carried, gate_in)
    keep = jnp.exp(carried - stab_next)
    write = jnp.exp(gate_in - stab_next)
    floor = jnp.exp(-stab_next)
    for h in range(heads):
        keep_v[:, h, :] = jnp.broadcast_to(keep[:, h : h + 1], (rows, 128))
        write_v[:, h, :] = jnp.broadcast_to(write[:, h : h + 1], (rows, 128))
        t_v[0:rows, h : h + 1] = stab_next[:, h : h + 1]
    stab_out[...] = t_v[...].T[0:heads, 0:rows]

    loads[7].wait()
    for ch in range(1, 3):
        cell_load(ch).start()
    query = jnp.dot(normed, wq_v[...], preferred_element_type=F32).astype(BF16).astype(F32)
    loads[8].wait()
    for ch in range(3, chunks):
        cell_load(ch).start()
    key = jnp.dot(normed, wk_v[...], preferred_element_type=F32).astype(BF16).astype(F32)
    pad = jnp.zeros((128 - rows, heads * dk), F32)
    kt_v[...] = jnp.concatenate([key, pad], axis=0).T
    loads[9].wait()
    value = jnp.dot(normed, wv_v[...], preferred_element_type=F32).astype(BF16).astype(F32)
    for h in range(heads):
        v_v[:, h, 0:dv] = value[:, dv * h : dv * h + dv]
        for ch in range(chunks):
            q_v[ch, h, 0:CHUNK, 0:dk] = query[ch * CHUNK : ch * CHUNK + CHUNK, dk * h : dk * h + dk]
    loads[10].wait()
    scale = dk ** (-0.5)
    for h in range(heads):
        fresh = keep[:, h : h + 1] * norm_v[:, h, :] + write[:, h : h + 1] * key[:, dk * h : dk * h + dk]
        norm_out[:, h, :] = fresh
        along = jnp.sum(query[:, dk * h : dk * h + dk] * scale * fresh, axis=-1, keepdims=True)
        den = jnp.maximum(jnp.abs(along), floor[:, h : h + 1])
        den_v[:, 128 * h : 128 * h + 128] = jnp.broadcast_to(den, (rows, 128))

    def serve(ch, carry):
        cell_load(ch).wait()
        shift = lax.rem(128 - ch * CHUNK, 128)
        for h in range(heads):
            kt = pltpu.roll(kt_v[dk * h : dk * h + dk, :], shift, 1)
            q = q_v[ch, h, :, 0:dk].astype(BF16)
            for j in range(CHUNK):
                b = ch * CHUNK + j
                kc = jnp.broadcast_to(kt[:, j : j + 1], (dk, 128))
                keep_b = keep_v[b, h : h + 1, :]
                write_b = write_v[b, h : h + 1, :]
                parts = []
                for lo, hi in ((0, 128), (128, dv)):
                    n = hi - lo
                    fed = write_b[:, :n] * v_v[b, h : h + 1, lo:hi]
                    fresh = keep_b[:, :n] * m_v[b, h, :, lo:hi] + kc[:, :n] * fed
                    m_v[b, h, :, lo:hi] = fresh
                    parts.append(fresh)
                fresh = jnp.concatenate(parts, axis=1)
                high = fresh.astype(BF16)
                low = (fresh - high.astype(F32)).astype(BF16)
                num = jnp.dot(q, high, preferred_element_type=F32) + jnp.dot(q, low, preferred_element_type=F32)
                num_v[b, h : h + 1, 0:dv] = num[j : j + 1, :]
        cell_store(ch).start()
        return carry

    lax.fori_loop(0, chunks, serve, 0)
    for h in range(heads):
        den = den_v[:, 128 * h : 128 * h + 128]
        wide = jnp.concatenate([den, den[:, : dv - 128]], axis=1)
        cell_v[h, :, :] = (num_v[:, h, 0:dv] * scale / wide).astype(BF16)
    given = pltpu.make_async_copy(cell_v, cell_out, in_sem.at[11])
    given.start()

    def drain(ch, carry):
        cell_store(ch).wait()
        return carry

    lax.fori_loop(0, chunks, drain, 0)
    given.wait()


def expert_kernel(
    cell, tok, wmix, gain_post, gain_ffn, wr, routes, wg, wu, wd, gain_last,
    mixed,
    cell_v, tok_v, wmix_v, gpost_v, gffn_v, wr_v, rt_v, glast_v, t_v, wg_v, wu_v, wd_v, send, xa, xb, own_part, part_send, part_recv, back_send, back,
    in_sem, send_s, send_r, fwd_s, fwd_r, part_s, part_r, back_s, back_r,
):
    me = lax.axis_index("ep")
    core, chip = lax.rem(me, 2), me // 2
    z, y, x = chip // 16, lax.rem(chip // 4, 4), lax.rem(chip, 4)
    partner = me + 1 - 2 * core

    def at(index, sign):
        dz, dy, dx = offset_of(index)
        if sign < 0:
            dz, dy, dx = -dz % 4, -dy % 4, -dx % 4
        return ((lax.rem(z + dz, 4) * 4 + lax.rem(y + dy, 4)) * 4 + lax.rem(x + dx, 4)) * 2 + core

    def cut(index):
        return pl.ds(SLOTS * index, SLOTS)

    barrier = pltpu.get_barrier_semaphore()
    for i in range(1, CHIPS):
        pl.semaphore_signal(barrier, inc=1, device_id=(at(i, 1),), device_id_type=MESH)
    pl.semaphore_signal(barrier, inc=1, device_id=(partner,), device_id_type=MESH)
    block = pl.multiple_of(me // 4 * 128, 128)
    pairs = [
        (tok, tok_v), (routes.at[:, pl.ds(block, 128)], rt_v), (wmix, wmix_v), (gain_post, gpost_v), (gain_ffn, gffn_v),
        (wr, wr_v), (gain_last, glast_v), (cell, cell_v), (wg.at[0], wg_v), (wu.at[0], wu_v), (wd.at[0], wd_v),
    ]
    loads = [pltpu.make_async_copy(s, d, in_sem.at[i]) for i, (s, d) in enumerate(pairs)]
    for copy in loads[:8]:
        copy.start()

    loads[0].wait()
    loads[1].wait()
    rows, (heads, _, dv) = tok_v.shape[0], cell.shape
    t_v[...] = jnp.zeros_like(t_v)
    t_v[0:2, :] = rt_v[...].astype(F32)
    t_v[...] = t_v[...].T
    own = t_v[pl.ds(pl.multiple_of(lax.rem(me, 4) * rows, rows), rows), :]
    first, second = own[:, 0:1], own[:, 1:2]
    lane = lax.broadcasted_iota(jnp.int32, (rows, LANES), 1)
    index = lane >> 2
    dy, dx = (index >> 2) & 3, index & 3
    dz = ((index >> 4) - dy - dx + 8) & 3
    expert = ((((z + dz) & 3) * 16 + ((y + dy) & 3) * 4 + ((x + dx) & 3)) >> 1).astype(F32)
    hit0 = (expert == first).astype(F32)
    hit1 = (expert == second).astype(F32)
    hot = hit0 + hit1
    before = lax.broadcasted_iota(jnp.int32, (rows, rows), 1) < lax.broadcasted_iota(jnp.int32, (rows, rows), 0)
    rank = jnp.dot(before.astype(F32).astype(BF16), hot.astype(BF16), preferred_element_type=F32)
    place = jnp.where(rank == (lane & 3).astype(F32), hot, 0.0)

    loads[2].wait()
    loads[7].wait()
    for copy in loads[8:]:
        copy.start()
    mix = jnp.zeros(tok_v.shape, F32)
    for h in range(heads):
        mix = mix + jnp.dot(cell_v[h], wmix_v[dv * h : dv * h + dv, :], preferred_element_type=F32)
    for i in range(3, 7):
        loads[i].wait()
    after = (tok_v[...].astype(F32) + rms(mix, gpost_v[...])).astype(BF16).astype(F32)
    expert_in = rms(after, gffn_v[...]).astype(BF16)
    tn = (((0,), (0,)), ((), ()))
    send[...] = lax.dot_general(place.astype(BF16), expert_in, tn, preferred_element_type=F32).astype(BF16)
    xa[0:SLOTS, :] = send[0:SLOTS, :]
    pl.semaphore_wait(barrier, CHIPS)

    def to_expert(i):
        return pltpu.make_async_remote_copy(
            src_ref=send.at[cut(i)], dst_ref=xa.at[cut(i)], send_sem=send_s.at[i], recv_sem=send_r.at[i],
            device_id=(at(i, 1),), device_id_type=MESH,
        )

    def to_source(i):
        return pltpu.make_async_remote_copy(
            src_ref=back_send.at[cut(i)], dst_ref=back.at[cut(i)], send_sem=back_s.at[i], recv_sem=back_r.at[i],
            device_id=(at(i, -1),), device_id_type=MESH,
        )

    def to_partner(src, dst, ssem, rsem, g):
        part = pl.ds(HALF * g, HALF)
        return pltpu.make_async_remote_copy(
            src_ref=src.at[part], dst_ref=dst.at[part], send_sem=ssem.at[g], recv_sem=rsem.at[g],
            device_id=(partner,), device_id_type=MESH,
        )

    order = list(range(GROUPS))[1:] + [0]
    for g in order:
        for i in range(PER * g, PER * g + PER):
            if i:
                to_expert(i).start()

    logits = lax.dot_general(expert_in, wr_v[...], NT, preferred_element_type=F32)
    ids = lax.broadcasted_iota(jnp.int32, logits.shape, 1).astype(F32)
    zero = jnp.zeros_like(logits)
    chosen0 = jnp.sum(jnp.where(ids == first, logits, zero), axis=-1, keepdims=True)
    chosen1 = jnp.sum(jnp.where(ids == second, logits, zero), axis=-1, keepdims=True)
    weight = place * (hit0 * jax.nn.sigmoid(chosen0 - chosen1) + hit1 * jax.nn.sigmoid(chosen1 - chosen0))
    high = weight.astype(BF16)
    low = (weight - high.astype(F32)).astype(BF16)
    for copy in loads[8:]:
        copy.wait()

    def finish(g):
        part = slice(HALF * g, HALF * g + HALF)
        to_partner(part_send, part_recv, part_s, part_r, g).wait_recv()
        back_send[part, :] = (own_part[part, :] + part_recv[part, :].astype(F32)).astype(BF16)
        for i in range(PER * g, PER * g + PER):
            if i:
                to_source(i).start()
            else:
                back[0:SLOTS, :] = back_send[0:SLOTS, :]

    last = None
    for g in order:
        part = slice(HALF * g, HALF * g + HALF)
        for i in range(PER * g, PER * g + PER):
            if i:
                to_expert(i).wait_recv()
        to_partner(xa, xb, fwd_s, fwd_r, g).start()
        if last is not None:
            finish(last)
        to_partner(xa, xb, fwd_s, fwd_r, g).wait_recv()
        block = jnp.concatenate([xa[part, :], xb[part, :]], axis=0)
        gate = jnp.dot(block, wg_v[...], preferred_element_type=F32)
        up = jnp.dot(block, wu_v[...], preferred_element_type=F32)
        hidden = (gate * jax.nn.sigmoid(gate) * up).astype(BF16)
        result = jnp.dot(hidden, wd_v[...], preferred_element_type=F32)
        part_send[part, :] = result[HALF:, :].astype(BF16)
        to_partner(part_send, part_recv, part_s, part_r, g).start()
        own_part[part, :] = result[:HALF, :]
        last = g
    finish(last)

    total = None
    for g in order:
        part = slice(HALF * g, HALF * g + HALF)
        for i in range(PER * g, PER * g + PER):
            if i:
                to_source(i).wait_recv()
        rows = back[part, :]
        more = jnp.dot(high[:, part], rows, preferred_element_type=F32)
        more = more + jnp.dot(low[:, part], rows, preferred_element_type=F32)
        total = more if total is None else total + more
    mixed[...] = (after + rms(total, glast_v[...])).astype(BF16)

    for i in range(1, CHIPS):
        to_expert(i).wait_send()
        to_source(i).wait_send()
    for g in range(GROUPS):
        to_partner(xa, xb, fwd_s, fwd_r, g).wait_send()
        to_partner(part_send, part_recv, part_s, part_r, g).wait_send()


def body(
    tokens, gain_mix, w_query, w_key, w_value, w_input_gate, w_forget_gate, bias_input, bias_forget, memory_cells,
    normalizer, stabilizer, w_mix_out, gain_mix_post, gain_ffn, w_router, routing, w_expert_gate, w_expert_up,
    w_expert_down, gain_ffn_post,
):
    rows, width = tokens.shape
    _, heads, dk, dv = memory_cells.shape
    hidden = w_expert_gate.shape[2]
    row = lambda v: v.reshape(1, -1)
    hbm, vmem = pl.BlockSpec(memory_space=pltpu.HBM), pl.BlockSpec(memory_space=pltpu.VMEM)
    shape = jax.ShapeDtypeStruct
    dma = pltpu.SemaphoreType.DMA
    like = lambda a: pltpu.VMEM(a.shape, a.dtype)
    front_in = (
        tokens, row(gain_mix), w_query, w_key, w_value, w_input_gate.T, w_forget_gate.T, row(bias_input),
        row(bias_forget), memory_cells, normalizer, stabilizer.T,
    )
    cells_next, norm_next, stab_next, cell = pl.pallas_call(
        front_kernel,
        out_shape=(
            shape(memory_cells.shape, F32), shape(normalizer.shape, F32), shape((heads, rows), F32),
            shape((heads, rows, dv), BF16),
        ),
        in_specs=[hbm] * len(front_in),
        out_specs=(hbm, vmem, vmem, hbm),
        scratch_shapes=[like(a) for a in front_in]
        + [
            pltpu.VMEM((heads, rows, dv), BF16),
            pltpu.VMEM((heads * dk, 128), F32), pltpu.VMEM((rows // CHUNK, heads, 8, 128), F32),
            pltpu.VMEM((rows, heads, 256), F32), pltpu.VMEM((rows, heads, 128), F32), pltpu.VMEM((rows, heads, 128), F32),
            pltpu.VMEM((rows, heads, 256), F32), pltpu.VMEM((rows, heads * 128), F32), pltpu.VMEM((128, 128), F32),
            dma((12,)), dma((rows // CHUNK,)), dma((rows // CHUNK,)),
        ],
        compiler_params=pltpu.CompilerParams(vmem_limit_bytes=VMEM_LIMIT),
        name="front",
    )(*front_in)

    big = pltpu.VMEM((LANES, width), BF16)
    router = w_router.T
    mixed = pl.pallas_call(
        expert_kernel,
        out_shape=pltpu.VMEM((rows, width), BF16),
        in_specs=[hbm] * 11,
        out_specs=vmem,
        scratch_shapes=[
            pltpu.VMEM((heads, rows, dv), BF16), like(tokens), like(w_mix_out), like(row(gain_mix_post)), like(row(gain_ffn)), like(router),
            pltpu.VMEM((2, 128), jnp.int32), like(row(gain_ffn_post)), pltpu.VMEM((128, 128), F32),
            pltpu.VMEM((width, hidden), BF16), pltpu.VMEM((width, hidden), BF16), pltpu.VMEM((hidden, width), BF16),
            big, big, big, pltpu.VMEM((LANES, width), F32), big, big, big, big,
            dma((11,)), dma((CHIPS,)), dma((CHIPS,)), dma((GROUPS,)), dma((GROUPS,)), dma((GROUPS,)), dma((GROUPS,)),
            dma((CHIPS,)), dma((CHIPS,)),
        ],
        compiler_params=pltpu.CompilerParams(collective_id=0, has_side_effects=True, vmem_limit_bytes=VMEM_LIMIT - 256 * 1024),
        name="experts",
    )(
        cell, tokens, w_mix_out, row(gain_mix_post), row(gain_ffn), router, routing.T, w_expert_gate, w_expert_up,
        w_expert_down, row(gain_ffn_post),
    )
    return (mixed, cells_next, norm_next, stab_next.T)


def solution(mesh):
    return jax.shard_map(
        body,
        mesh=mesh,
        in_specs=(
            P("ep", None),
            P(),
            P(),
            P(),
            P(),
            P(),
            P(),
            P(),
            P(),
            P("ep", None, None, None),
            P("ep", None, None),
            P("ep", None),
            P(),
            P(),
            P(),
            P(),
            P(),
            P("ep", None, None),
            P("ep", None, None),
            P("ep", None, None),
            P(),
        ),
        out_specs=(P("ep", None), P("ep", None, None, None), P("ep", None, None), P("ep", None)),
        check_vma=False,
    )
```

time: 61.2 us -> 55.1 us (0.900)
  Pallas kernels: 58.9 us -> 53.6 us
  local copies, waits for them, and re-layouts: 1.57 us -> 0.66 us
    pallas_call x1, Pallas kernels: 15.9 us -> 11.9 us  [body(): pl.pallas_call(front_kernel, out_shape=(shape(memory_cells.shape, F32), s...]
    pallas_call x1, Pallas kernels: 43 us -> 41.8 us  [body(): pl.pallas_call(expert_kernel, out_shape=pltpu.VMEM((rows, width), BF16),...]
    unnamed x1, local copies, waits for them, and re-layouts: 1.57 us -> 0.66 us
where the time goes in v2:
time: 55.1 us; the launch traced here: 54.9 us
  Pallas kernels  53.6 us (97%)
  local copies, waits for them, and re-layouts  0.66 us (1%)
  between operations  0.65 us (1%)
    pallas_call x1, Pallas kernels, body(): pl.pallas_call(expert_kernel, out_shape=pltpu.VMEM((rows, width), BF16),...  41.8 us
    pallas_call x1, Pallas kernels, body(): pl.pallas_call(front_kernel, out_shape=(shape(memory_cells.shape, F32), s...  11.9 us

profile of v2, /device:TPU:1, one launch (start us, length us, event | category | flops | bytes accessed | tf_op | source)
XLA Modules:
  0.0 54.9 jit_solution(13597622464703815423)
XLA Ops:
  0.6 11.9 %front.1 = (f32[32,4,96,192]{3,2,1,0:T(8,128)}, f32[32,4,96]{2,1,0:T(4,128)}, f32[4,32]{1,0:T(4,128)}, bf16[4,32,192]{2,1,0:T(8,128)(2,1)}) custom-call(bf16[32,2048]{1,0:T(8,128)(2,1)} %tok.3, f32[1,2048]{1,0:T(1,128)} %bitcast.16, bf16[2048,384]{1,0:T(8,128)(2,1)} %wq.1, bf16[2048,384]{1,0:T(8,128)(2,1)} %wk.1, bf16[2048,768]{1,0:T(8,128)(2,1)} %wv.1, ...), custom_call_target="tpu_custom_call" | custom-call | tf_op jit(solution)/shard_map/front/pallas_call | solution.py:324
  12.5 41.8 %experts.1 = bf16[32,2048]{1,0:T(8,128)(2,1)S(1)} custom-call(bf16[4,32,192]{2,1,0:T(8,128)(2,1)} %get-tuple-element.8.cell, bf16[32,2048]{1,0:T(8,128)(2,1)} %tok.3, bf16[768,2048]{1,0:T(8,128)(2,1)} %wmix.1, f32[1,2048]{1,0:T(1,128)} %bitcast.17, f32[1,2048]{1,0:T(1,128)} %bitcast.18, bf16[32,2048]{1,0:T(8,128)(2,1)} %bitcast.12, s32[2,4096]{1,0:T(2,128)} %bitcast.13, ...), custom_call_target="tpu_custom_call" | custom-call | tf_op jit(solution)/shard_map/experts/pallas_call | solution.py:346
  54.3 0.7 %copy.26 = bf16[32,2048]{1,0:T(8,128)(2,1)} copy(bf16[32,2048]{1,0:T(8,128)(2,1)S(1)} %experts.1) | data formatting | bytes 262144

commit v3 on v2

--- a/solution.py
+++ b/solution.py
@@ -20,7 +20,7 @@
 LANES = CHIPS * SLOTS
 HALF = LANES // GROUPS
 NT = (((1,), (1,)), ((), ()))
-CHUNK = 4
+CHUNK = 8
 
 
 def rms(values, gain):
@@ -31,6 +31,10 @@
 def offset_of(index):
     g, dy, dx = index // PER, index // 4 % 4, index % 4
     return (g - dy - dx) % 4, dy, dx
+
+
+def hops(index):
+    return sum(min(v, 4 - v) for v in offset_of(index))
 
 
 def front_kernel(
@@ -82,11 +86,11 @@
     stab_out[...] = t_v[...].T[0:heads, 0:rows]
 
     loads[7].wait()
-    for ch in range(1, 3):
+    for ch in range(1, 2):
         cell_load(ch).start()
     query = jnp.dot(normed, wq_v[...], preferred_element_type=F32).astype(BF16).astype(F32)
     loads[8].wait()
-    for ch in range(3, chunks):
+    for ch in range(2, chunks):
         cell_load(ch).start()
     key = jnp.dot(normed, wk_v[...], preferred_element_type=F32).astype(BF16).astype(F32)
     pad = jnp.zeros((128 - rows, heads * dk), F32)
@@ -169,7 +173,7 @@
         return pl.ds(SLOTS * index, SLOTS)
 
     barrier = pltpu.get_barrier_semaphore()
-    for i in range(1, CHIPS):
+    for i in sorted(range(1, CHIPS), key=lambda i: -hops(i)):
         pl.semaphore_signal(barrier, inc=1, device_id=(at(i, 1),), device_id_type=MESH)
     pl.semaphore_signal(barrier, inc=1, device_id=(partner,), device_id_type=MESH)
     block = pl.multiple_of(me // 4 * 128, 128)
@@ -236,9 +240,9 @@
             device_id=(partner,), device_id_type=MESH,
         )
 
-    order = list(range(GROUPS))[1:] + [0]
+    order = [2, 1, 3, 0]
     for g in order:
-        for i in range(PER * g, PER * g + PER):
+        for i in sorted(range(PER * g, PER * g + PER), key=lambda i: -hops(i)):
             if i:
                 to_expert(i).start()
 

time: 55.1 us -> 53.3 us (0.967)
  Pallas kernels: 53.6 us -> 51.9 us
    pallas_call x1, Pallas kernels: 41.8 us -> 40.7 us  [body(): pl.pallas_call(expert_kernel, out_shape=pltpu.VMEM((rows, width), BF16),...]
    pallas_call x1, Pallas kernels: 11.9 us -> 11.2 us  [body(): pl.pallas_call(front_kernel, out_shape=(shape(memory_cells.shape, F32), s...]
where the time goes in v3:
time: 53.3 us; the launch traced here: 53.2 us
  Pallas kernels  51.9 us (97%)
  local copies, waits for them, and re-layouts  0.66 us (1%)
  between operations  0.65 us (1%)
    pallas_call x1, Pallas kernels, body(): pl.pallas_call(expert_kernel, out_shape=pltpu.VMEM((rows, width), BF16),...  40.7 us
    pallas_call x1, Pallas kernels, body(): pl.pallas_call(front_kernel, out_shape=(shape(memory_cells.shape, F32), s...  11.2 us

profile of v3, /device:TPU:1, one launch (start us, length us, event | category | flops | bytes accessed | tf_op | source)
XLA Modules:
  0.0 53.2 jit_solution(7857240212913458940)
XLA Ops:
  0.6 11.2 %front.1 = (f32[32,4,96,192]{3,2,1,0:T(8,128)}, f32[32,4,96]{2,1,0:T(4,128)}, f32[4,32]{1,0:T(4,128)}, bf16[4,32,192]{2,1,0:T(8,128)(2,1)}) custom-call(bf16[32,2048]{1,0:T(8,128)(2,1)} %tok.3, f32[1,2048]{1,0:T(1,128)} %bitcast.16, bf16[2048,384]{1,0:T(8,128)(2,1)} %wq.1, bf16[2048,384]{1,0:T(8,128)(2,1)} %wk.1, bf16[2048,768]{1,0:T(8,128)(2,1)} %wv.1, ...), custom_call_target="tpu_custom_call" | custom-call | tf_op jit(solution)/shard_map/front/pallas_call | solution.py:328
  11.8 40.7 %experts.1 = bf16[32,2048]{1,0:T(8,128)(2,1)S(1)} custom-call(bf16[4,32,192]{2,1,0:T(8,128)(2,1)} %get-tuple-element.8.cell, bf16[32,2048]{1,0:T(8,128)(2,1)} %tok.3, bf16[768,2048]{1,0:T(8,128)(2,1)} %wmix.1, f32[1,2048]{1,0:T(1,128)} %bitcast.17, f32[1,2048]{1,0:T(1,128)} %bitcast.18, bf16[32,2048]{1,0:T(8,128)(2,1)} %bitcast.12, s32[2,4096]{1,0:T(2,128)} %bitcast.13, ...), custom_call_target="tpu_custom_call" | custom-call | tf_op jit(solution)/shard_map/experts/pallas_call | solution.py:350
  52.5 0.7 %copy.26 = bf16[32,2048]{1,0:T(8,128)(2,1)} copy(bf16[32,2048]{1,0:T(8,128)(2,1)S(1)} %experts.1) | data formatting | bytes 262144

commit v4 on v3

--- a/solution.py
+++ b/solution.py
@@ -261,7 +261,7 @@
         part = slice(HALF * g, HALF * g + HALF)
         to_partner(part_send, part_recv, part_s, part_r, g).wait_recv()
         back_send[part, :] = (own_part[part, :] + part_recv[part, :].astype(F32)).astype(BF16)
-        for i in range(PER * g, PER * g + PER):
+        for i in sorted(range(PER * g, PER * g + PER), key=lambda i: -hops(i)):
             if i:
                 to_source(i).start()
             else:

time: 53.3 us -> 52.4 us (0.983)
  Pallas kernels: 51.9 us -> 51 us
    pallas_call x1, Pallas kernels: 40.7 us -> 39.8 us  [body(): pl.pallas_call(expert_kernel, out_shape=pltpu.VMEM((rows, width), BF16),...]
where the time goes in v4:
time: 52.4 us; the launch traced here: 52.3 us
  Pallas kernels  51 us (97%)
  local copies, waits for them, and re-layouts  0.66 us (1%)
  between operations  0.65 us (1%)
    pallas_call x1, Pallas kernels, body(): pl.pallas_call(expert_kernel, out_shape=pltpu.VMEM((rows, width), BF16),...  39.8 us
    pallas_call x1, Pallas kernels, body(): pl.pallas_call(front_kernel, out_shape=(shape(memory_cells.shape, F32), s...  11.2 us

profile of v4, /device:TPU:1, one launch (start us, length us, event | category | flops | bytes accessed | tf_op | source)
XLA Modules:
  0.0 52.3 jit_solution(17331883511434456551)
XLA Ops:
  0.6 11.2 %front.1 = (f32[32,4,96,192]{3,2,1,0:T(8,128)}, f32[32,4,96]{2,1,0:T(4,128)}, f32[4,32]{1,0:T(4,128)}, bf16[4,32,192]{2,1,0:T(8,128)(2,1)}) custom-call(bf16[32,2048]{1,0:T(8,128)(2,1)} %tok.3, f32[1,2048]{1,0:T(1,128)} %bitcast.16, bf16[2048,384]{1,0:T(8,128)(2,1)} %wq.1, bf16[2048,384]{1,0:T(8,128)(2,1)} %wk.1, bf16[2048,768]{1,0:T(8,128)(2,1)} %wv.1, ...), custom_call_target="tpu_custom_call" | custom-call | tf_op jit(solution)/shard_map/front/pallas_call | solution.py:328
  11.8 39.8 %experts.1 = bf16[32,2048]{1,0:T(8,128)(2,1)S(1)} custom-call(bf16[4,32,192]{2,1,0:T(8,128)(2,1)} %get-tuple-element.8.cell, bf16[32,2048]{1,0:T(8,128)(2,1)} %tok.3, bf16[768,2048]{1,0:T(8,128)(2,1)} %wmix.1, f32[1,2048]{1,0:T(1,128)} %bitcast.17, f32[1,2048]{1,0:T(1,128)} %bitcast.18, bf16[32,2048]{1,0:T(8,128)(2,1)} %bitcast.12, s32[2,4096]{1,0:T(2,128)} %bitcast.13, ...), custom_call_target="tpu_custom_call" | custom-call | tf_op jit(solution)/shard_map/experts/pallas_call | solution.py:350
  51.7 0.7 %copy.26 = bf16[32,2048]{1,0:T(8,128)(2,1)} copy(bf16[32,2048]{1,0:T(8,128)(2,1)S(1)} %experts.1) | data formatting | bytes 262144
